TPU v7x, 32 devices: a whole 2x2x4 slice. The times are simulated.
32 devices in a mesh: ep: 8 (over z, y), tp: 4 (over x, core).
Axes of the slice: x: 2, y: 2, z: 4, core: 2. Of those that a mesh axis runs over, the one named last changes fastest.
Arguments:
- queries: bfloat16 [4096, 1024], P('ep', 'tp'), may hold values from -6 to 6
- keys: bfloat16 [4096, 512], P('ep', 'tp'), may hold values from -6 to 6
- values: bfloat16 [4096, 512], P('ep', 'tp'), may hold values from -384 to 384
- query_gain: float32 [128], replicated, may hold values from 0.1 to 1.9
- key_gain: float32 [128], replicated, may hold values from 0.1 to 1.9
- out_proj: bfloat16 [1024, 2048], replicated, may hold values from -0.1875 to 0.1875
- tokens_b: bfloat16 [4096, 2048], P(('ep', 'tp')), may hold values from -6 to 6
- norm_gain: float32 [2048], replicated, may hold values from 0.1 to 1.9
- routes: int32 [4096, 2], P(('ep', 'tp')), may hold values from 0 to 31, all different within a row; in each aligned block of 128 rows (0 to 127, 128 to 255, ...) at most 16 rows name the same one
- group_prob: float32 [4096], P(('ep', 'tp')), may hold values from 0.25 to 1
- expert_logits: float32 [4096, 2], P(('ep', 'tp')), may hold values from -6 to 6
- w_gate: bfloat16 [32, 2048, 512], P(('ep', 'tp')), may hold values from -0.125 to 0.125
- w_up: bfloat16 [32, 2048, 512], P(('ep', 'tp')), may hold values from -0.125 to 0.125
- w_down: bfloat16 [32, 512, 2048], P(('ep', 'tp')), may hold values from -0.25 to 0.25
Outputs:
- mixed_a: bfloat16 [4096, 2048], P(('ep', 'tp'))
- mixed_b: bfloat16 [4096, 2048], P(('ep', 'tp'))
Inputs may be any that keep to these rules, and one draw needn't show every extreme that they name: Within the 128 rows of one device, no expert is named by more than 16 of the routes, and in every draw some expert is named exactly 16 times by the rows of some device. The 2 experts of a row differ.
All inputs are finite; a program needn't handle non-finite values.
Results may differ from a plain program's by a relative error of at most 0.014.
Values may be sent and summed in bfloat16 or wider, within the bound.
A program may use at most 128 MiB of HBM per device.

v0:
```python
import math
import jax
import jax.numpy as jnp
from jax import lax
from jax.sharding import PartitionSpec as P

GRID_W = 64
NORM_EPS = 1e-06
ROPE_BASE = 10000.0


def rope_angles(row_count, offset, head_dim):
    quarter = head_dim // 4
    position = offset + jnp.arange(row_count, dtype=jnp.int32)
    grid_row = (position // GRID_W).astype(jnp.float32)
    grid_col = (position % GRID_W).astype(jnp.float32)
    frequency = ROPE_BASE ** (-jnp.arange(quarter, dtype=jnp.float32) / quarter)
    angles = jnp.concatenate([grid_row[:, None] * frequency, grid_col[:, None] * frequency], axis=1)
    return (jnp.cos(angles), jnp.sin(angles))


def norm_rotate(block_in, gain, cos_table, sin_table):
    wide = block_in.astype(jnp.float32)
    wide = wide * lax.rsqrt(jnp.mean(wide * wide, axis=-1, keepdims=True) + NORM_EPS) * gain
    half_width = wide.shape[-1] // 2
    first_half, second_half = (wide[..., :half_width], wide[..., half_width:])
    cos_b = cos_table[:, None, :]
    sin_b = sin_table[:, None, :]
    turned = jnp.concatenate(
        [first_half * cos_b - second_half * sin_b, second_half * cos_b + first_half * sin_b],
        axis=-1,
    )
    return turned.astype(jnp.bfloat16)


def attention_half(queries, keys, values, query_gain, key_gain, out_proj):
    row_count = queries.shape[0]
    head_dim = query_gain.shape[0]
    local_heads = queries.shape[1] // head_dim
    local_kv = keys.shape[1] // head_dim
    group_size = local_heads // local_kv
    offset = lax.axis_index("ep") * row_count
    cos_table, sin_table = rope_angles(row_count, offset, head_dim)
    qrot = norm_rotate(
        queries.reshape(row_count, local_heads, head_dim), query_gain, cos_table, sin_table
    )
    qrot = qrot.reshape(row_count, local_kv, group_size, head_dim)
    krot = norm_rotate(keys.reshape(row_count, local_kv, head_dim), key_gain, cos_table, sin_table)
    krot = krot.reshape(row_count, local_kv * head_dim)
    score_scale = head_dim ** (-0.5)
    start_pair = (
        jnp.zeros((row_count, local_kv, group_size, head_dim), jnp.float32),
        jnp.zeros((row_count, local_kv, group_size), jnp.float32),
    )
    key_piece = lax.all_gather(krot, "ep", axis=0, tiled=True)
    value_piece = lax.all_gather(values, "ep", axis=0, tiled=True)
    piece_rows = key_piece.shape[0]
    key_block = math.gcd(piece_rows, 1024)
    block_count = piece_rows // key_block
    key_tiles = key_piece.reshape(block_count, key_block, local_kv, head_dim)
    value_tiles = value_piece.reshape(block_count, key_block, local_kv, head_dim)

    def key_step(pair, tiles):
        numerator, denominator = pair
        key_tile, value_tile = tiles
        scores = (
            jnp.einsum("qhgd,khd->qhgk", qrot, key_tile, preferred_element_type=jnp.float32)
            * score_scale
        )
        weights = jnp.exp(scores).astype(jnp.bfloat16)
        denominator = denominator + jnp.sum(weights.astype(jnp.float32), axis=-1)
        numerator = numerator + jnp.einsum(
            "qhgk,khd->qhgd", weights, value_tile, preferred_element_type=jnp.float32
        )
        return ((numerator, denominator), None)

    numerator, denominator = lax.scan(key_step, start_pair, (key_tiles, value_tiles))[0]
    attended = (
        (numerator / denominator[..., None])
        .astype(jnp.bfloat16)
        .reshape(row_count, local_heads * head_dim)
    )
    own_width = local_heads * head_dim
    own_rows = lax.dynamic_slice_in_dim(out_proj, lax.axis_index("tp") * own_width, own_width, 0)
    return lax.psum_scatter(
        jnp.dot(attended, own_rows, preferred_element_type=jnp.float32).astype(jnp.bfloat16),
        "tp",
        scatter_dimension=0,
        tiled=True,
    )


def expert_apply(inputs, gate_w, up_w, down_w):
    gate_part = jnp.dot(inputs, gate_w, preferred_element_type=jnp.float32)
    up_part = jnp.dot(inputs, up_w, preferred_element_type=jnp.float32)
    hidden = (jax.nn.silu(gate_part) * up_part).astype(jnp.bfloat16)
    return jnp.dot(hidden, down_w, preferred_element_type=jnp.float32).astype(jnp.bfloat16)


def expert_half(tokens_b, norm_gain, routes, group_prob, expert_logits, w_gate, w_up, w_down):
    ep_count = lax.axis_size("ep")
    tp_count = lax.axis_size("tp")
    device_count = ep_count * tp_count
    row_count, top_count = routes.shape
    model_width = tokens_b.shape[1]
    capacity = 2 * top_count * row_count // device_count
    wide_b = tokens_b.astype(jnp.float32)
    normed = (
        wide_b * lax.rsqrt(jnp.mean(wide_b * wide_b, axis=-1, keepdims=True) + NORM_EPS) * norm_gain
    ).astype(jnp.bfloat16)
    flat_routes = routes.reshape(-1)
    onehot = (flat_routes[:, None] == jnp.arange(device_count, dtype=jnp.int32)[None, :]).astype(
        jnp.int32
    )
    slot_rank = jnp.sum((jnp.cumsum(onehot, axis=0) - onehot) * onehot, axis=1)
    target_slot = flat_routes * capacity + slot_rank
    token_index = jnp.arange(row_count * top_count, dtype=jnp.int32) // top_count
    sender = (
        jnp.zeros((device_count * capacity, model_width), jnp.bfloat16)
        .at[target_slot]
        .set(normed[token_index])
    )
    arrived = lax.all_to_all(
        sender.reshape(device_count, capacity, model_width),
        ("ep", "tp"),
        split_axis=0,
        concat_axis=0,
        tiled=True,
    )
    expert_out = expert_apply(
        arrived.reshape(device_count * capacity, model_width), w_gate[0], w_up[0], w_down[0]
    )
    returned = lax.all_to_all(
        expert_out.reshape(device_count, capacity, model_width),
        ("ep", "tp"),
        split_axis=0,
        concat_axis=0,
        tiled=True,
    )
    returned = returned.reshape(device_count * capacity, model_width)
    picked = returned[target_slot].reshape(row_count, top_count, model_width).astype(jnp.float32)
    combine = group_prob[:, None] * jax.nn.softmax(expert_logits, axis=-1)
    return jnp.sum(picked * combine[:, :, None], axis=1).astype(jnp.bfloat16)


def body(
    queries,
    keys,
    values,
    query_gain,
    key_gain,
    out_proj,
    tokens_b,
    norm_gain,
    routes,
    group_prob,
    expert_logits,
    w_gate,
    w_up,
    w_down,
):
    mixed_a = attention_half(queries, keys, values, query_gain, key_gain, out_proj)
    mixed_b = expert_half(
        tokens_b, norm_gain, routes, group_prob, expert_logits, w_gate, w_up, w_down
    )
    return (mixed_a, mixed_b)


def solution(mesh):
    placed = (
        P("ep", "tp"),
        P("ep", "tp"),
        P("ep", "tp"),
        P(),
        P(),
        P(),
        P(("ep", "tp"), None),
        P(),
        P(("ep", "tp"), None),
        P(("ep", "tp")),
        P(("ep", "tp"), None),
        P(("ep", "tp"), None, None),
        P(("ep", "tp"), None, None),
        P(("ep", "tp"), None, None),
    )
    return jax.shard_map(
        body,
        mesh=mesh,
        in_specs=placed,
        out_specs=(P(("ep", "tp"), None), P(("ep", "tp"), None)),
        check_vma=False,
    )
```

profile of v0, /device:TPU:0, one launch (start us, length us, event | category | flops | bytes accessed | tf_op | source)
XLA Modules:
  0.0 214.3 jit_solution(13210312035628791452)
XLA Ops:
  7.3 1.2 copy.30
  8.5 0.7 fusion.40
  13.4 7.0 %scatter_custom_fusion = bf16[512,2048]{1,0:T(8,128)(2,1)} fusion(s32[256]{0:T(256)S(1)} %bitcast.124, bf16[128,2048]{1,0:T(8,128)(2,1)S(1)} %fusion.28, s32[1024]{0:T(1024)S(1)} %pad_clamp_fusion.1, bf16[]{:T(256)} %constant.102.clone.1), kind=kCustom, calls=%fused_computation.32 | custom fusion | bytes 2097154 | tf_op jit(solution)/shard_map/scatter | solution.py:121
  20.4 7.6 %all-to-all-start = ((bf16[32,16,2048]{2,1,0:T(8,128)(2,1)}), bf16[32,16,2048]{2,1,0:T(8,128)(2,1)}, u32[]{:S(2)}, u32[]{:S(2)}) async-start(bf16[32,16,2048]{2,1,0:T(8,128)(2,1)} %bitcast.118), calls=%async_computation.1 | async-start | bytes 4194304 | tf_op jit(solution)/shard_map/all_to_all | solution.py:123
  29.2 39.7 %all-gather.5.cloned.1.call-done = bf16[4096,128]{0,1:T(8,128)(2,1)} async-done(((bf16[512,128]{0,1:T(8,128)(2,1)}), bf16[4096,128]{0,1:T(8,128)(2,1)}) %all-gather.5.cloned.1.call-update) | async-done | bytes 1048592 | tf_op jit(solution)/shard_map/all_gather | solution.py:55
  68.8 2.3 %copy.41 = bf16[4096,128]{1,0:T(8,128)(2,1)} copy(bf16[4096,128]{0,1:T(8,128)(2,1)} %all-gather.5.cloned.1.call-done) | data formatting | bytes 2097152
  71.1 40.1 %all-gather.3.cloned.1.call-done = bf16[4096,128]{1,0:T(8,128)(2,1)} async-done(((bf16[512,128]{1,0:T(8,128)(2,1)}), bf16[4096,128]{1,0:T(8,128)(2,1)}) %all-gather.3.cloned.1.call-update) | async-done | bytes 1048592 | tf_op jit(solution)/shard_map/all_gather | solution.py:56
  111.2 21.3 %while.13 = (s32[]{:T(128)}, f32[512,1,2,128]{0,3,2,1:T(8,128)S(1)}, f32[512,1,2]{0,2,1:T(2,128)S(1)}, bf16[4,1024,1,128]{3,1,0,2:T(8,128)(2,1)}, bf16[4,1024,1,...) while((s32[]{:T(128)}, ...), condition=%wide.region_4.5_spmd.clone, body=%wide.region_2.4_spmd.clone.sunk | while | flops 541328384 | bytes 6046816 | solution.py:77
  111.2 3.1 %convert_reduce_fusion.2 = (f32[512,2]{0,1:T(2,128)S(1)}, bf16[1024,512,2]{1,0,2:T(8,128)(2,1)}) fusion(bf16[512,1,2,128]{3,0,2,1:T(8,128)(2,1)S(1)} %get-tuple-element.160, bf16[4,1024,1,128]{3,1,2,0:T(8,128)(2,1)} %get-tuple-element.159, s32[]{:T(128)} %get-tuple-element.147), kind=kOutput, calls=%fused_computation.3.clone.1 | convolution fusion | flops 272628736 | bytes 2626048 | tf_op jit(solution)/shard_map/while/body/eval_jaxpr/qhgd,khd->qhgk/dot_general | solution.py:67
  114.3 2.2 %fusion.71 = f32[512,1,2,128]{0,3,2,1:T(8,128)S(1)} fusion(bf16[1024,512,2]{1,0,2:T(8,128)(2,1)} %get-tuple-element.137, f32[512,1,2,128]{0,3,2,1:T(8,128)S(1)} %get-tuple-element.148, bf16[4,1024,1,128]{3,1,0,2:T(8,128)(2,1)} %get-tuple-element.158, s32[]{:T(128)} %get-tuple-element.147, pred[]{:T(512)S(6)} %compare.18), kind=kOutput, calls=%fused_computation.8.clone.1 | convolution fusion | flops 268697600 | bytes 3408385 | tf_op jit(solution)/shard_map/while/body/eval_jaxpr/qhgk,khd->qhgd/dot_general | solution.py:72
  116.6 3.1 %convert_reduce_fusion.2 = (f32[512,2]{0,1:T(2,128)S(1)}, bf16[1024,512,2]{1,0,2:T(8,128)(2,1)}) fusion(bf16[512,1,2,128]{3,0,2,1:T(8,128)(2,1)S(1)} %get-tuple-element.160, bf16[4,1024,1,128]{3,1,2,0:T(8,128)(2,1)} %get-tuple-element.159, s32[]{:T(128)} %get-tuple-element.147), kind=kOutput, calls=%fused_computation.3.clone.1 | convolution fusion | flops 272628736 | bytes 2626048 | tf_op jit(solution)/shard_map/while/body/eval_jaxpr/qhgd,khd->qhgk/dot_general | solution.py:67
  119.7 2.2 %fusion.71 = f32[512,1,2,128]{0,3,2,1:T(8,128)S(1)} fusion(bf16[1024,512,2]{1,0,2:T(8,128)(2,1)} %get-tuple-element.137, f32[512,1,2,128]{0,3,2,1:T(8,128)S(1)} %get-tuple-element.148, bf16[4,1024,1,128]{3,1,0,2:T(8,128)(2,1)} %get-tuple-element.158, s32[]{:T(128)} %get-tuple-element.147, pred[]{:T(512)S(6)} %compare.18), kind=kOutput, calls=%fused_computation.8.clone.1 | convolution fusion | flops 268697600 | bytes 3408385 | tf_op jit(solution)/shard_map/while/body/eval_jaxpr/qhgk,khd->qhgd/dot_general | solution.py:72
  121.9 3.1 %convert_reduce_fusion.2 = (f32[512,2]{0,1:T(2,128)S(1)}, bf16[1024,512,2]{1,0,2:T(8,128)(2,1)}) fusion(bf16[512,1,2,128]{3,0,2,1:T(8,128)(2,1)S(1)} %get-tuple-element.160, bf16[4,1024,1,128]{3,1,2,0:T(8,128)(2,1)} %get-tuple-element.159, s32[]{:T(128)} %get-tuple-element.147), kind=kOutput, calls=%fused_computation.3.clone.1 | convolution fusion | flops 272628736 | bytes 2626048 | tf_op jit(solution)/shard_map/while/body/eval_jaxpr/qhgd,khd->qhgk/dot_general | solution.py:67
  125.0 2.2 %fusion.71 = f32[512,1,2,128]{0,3,2,1:T(8,128)S(1)} fusion(bf16[1024,512,2]{1,0,2:T(8,128)(2,1)} %get-tuple-element.137, f32[512,1,2,128]{0,3,2,1:T(8,128)S(1)} %get-tuple-element.148, bf16[4,1024,1,128]{3,1,0,2:T(8,128)(2,1)} %get-tuple-element.158, s32[]{:T(128)} %get-tuple-element.147, pred[]{:T(512)S(6)} %compare.18), kind=kOutput, calls=%fused_computation.8.clone.1 | convolution fusion | flops 268697600 | bytes 3408385 | tf_op jit(solution)/shard_map/while/body/eval_jaxpr/qhgk,khd->qhgd/dot_general | solution.py:72
  127.2 3.1 %convert_reduce_fusion.2 = (f32[512,2]{0,1:T(2,128)S(1)}, bf16[1024,512,2]{1,0,2:T(8,128)(2,1)}) fusion(bf16[512,1,2,128]{3,0,2,1:T(8,128)(2,1)S(1)} %get-tuple-element.160, bf16[4,1024,1,128]{3,1,2,0:T(8,128)(2,1)} %get-tuple-element.159, s32[]{:T(128)} %get-tuple-element.147), kind=kOutput, calls=%fused_computation.3.clone.1 | convolution fusion | flops 272628736 | bytes 2626048 | tf_op jit(solution)/shard_map/while/body/eval_jaxpr/qhgd,khd->qhgk/dot_general | solution.py:67
  130.3 2.2 %fusion.71 = f32[512,1,2,128]{0,3,2,1:T(8,128)S(1)} fusion(bf16[1024,512,2]{1,0,2:T(8,128)(2,1)} %get-tuple-element.137, f32[512,1,2,128]{0,3,2,1:T(8,128)S(1)} %get-tuple-element.148, bf16[4,1024,1,128]{3,1,0,2:T(8,128)(2,1)} %get-tuple-element.158, s32[]{:T(128)} %get-tuple-element.147, pred[]{:T(512)S(6)} %compare.18), kind=kOutput, calls=%fused_computation.8.clone.1 | convolution fusion | flops 268697600 | bytes 3408385 | tf_op jit(solution)/shard_map/while/body/eval_jaxpr/qhgk,khd->qhgd/dot_general | solution.py:72
  132.6 4.4 %fusion.18 = f32[512,512]{1,0:T(8,128)} fusion(bf16[512,2048]{1,0:T(8,128)(2,1)} %bitcast.18, bf16[1,2048,512]{2,1,0:T(8,128)(2,1)} %param.27), kind=kOutput, calls=%fused_computation.22 | convolution fusion | flops 1073741824 | bytes 5242880 | tf_op jit(solution)/shard_map/dot_general | solution.py:94
  137.1 6.2 %convolution_convert_fusion.1 = bf16[512,2048]{1,0:T(8,128)(2,1)} fusion(bf16[1,512,2048]{2,1,0:T(8,128)(2,1)S(1)} %copy-done, bf16[512,2048]{1,0:T(8,128)(2,1)} %bitcast.18, bf16[1,2048,512]{2,1,0:T(8,128)(2,1)} %param.28, f32[512,512]{1,0:T(8,128)} %fusion.18), kind=kOutput, calls=%fused_computation.18 | convolution fusion | flops 2150105088 | bytes 9437184 | tf_op jit(solution)/shard_map/dot_general | solution.py:97
  143.3 3.5 %all-to-all-start.1 = ((bf16[32,16,2048]{2,1,0:T(8,128)(2,1)}), bf16[32,16,2048]{2,1,0:T(8,128)(2,1)}, u32[]{:S(2)}, u32[]{:S(2)}) async-start(bf16[32,16,2048]{2,1,0:T(8,128)(2,1)} %bitcast.119), calls=%async_computation.2 | async-start | bytes 4194304 | tf_op jit(solution)/shard_map/all_to_all | solution.py:133
  147.1 3.3 %convolution_convert_fusion = bf16[512,2048]{1,0:T(8,128)(2,1)} fusion(bf16[512,256]{0,1:T(8,128)(2,1)S(1)} %bitcast.121, bf16[1024,2048]{1,0:T(8,128)(2,1)} %param.21, s32[]{:T(128)S(6)} %select_n.58), kind=kOutput, calls=%fused_computation.17 | convolution fusion | flops 537919488 | bytes 3407876 | tf_op jit(solution)/shard_map/dot_general | solution.py:86
  151.2 44.4 %all-to-all-done.1 = bf16[32,16,2048]{2,1,0:T(8,128)(2,1)} async-done(((bf16[32,16,2048]{2,1,0:T(8,128)(2,1)}), bf16[32,16,2048]{2,1,0:T(8,128)(2,1)}, u32[]{:S(2)}, u32[]{:S(2)}) %all-to-all-start.1) | async-done | bytes 2097184 | tf_op jit(solution)/shard_map/all_to_all | solution.py:133
  195.6 4.2 %gather_fusion = bf16[256,2048]{1,0:T(8,128)(2,1)S(1)} fusion(bf16[512,2048]{1,0:T(8,128)(2,1)} %bitcast.23, s32[1024]{0:T(1024)S(1)} %pad_clamp_fusion), kind=kCustom, calls=%fused_computation.1 | custom fusion | bytes 2098176 | tf_op jit(solution)/shard_map/gather | solution.py:141
  199.8 2.3 %reshape.420 = f32[128,2,2048]{2,1,0:T(2,128)} reshape(bf16[256,2048]{1,0:T(8,128)(2,1)S(1)} %gather_fusion) | data formatting | bytes 3145728 | tf_op jit(solution)/shard_map/convert_element_type | solution.py:141
  202.2 5.6 %multiply_reduce_fusion = bf16[128,2048]{1,0:T(8,128)(2,1)} fusion(f32[128,2,2048]{2,1,0:T(2,128)} %reshape.420, f32[128,2]{1,0:T(8,128)S(1)} %copy.39), kind=kLoop, calls=%fused_computation.24 | loop fusion | flops 786432 | bytes 2622464 | tf_op jit(solution)/shard_map/reduce_sum | solution.py:143
  (69 shorter events, 6.4 us)
Async XLA Ops:
  7.2 129.9 %copy-start = (bf16[1,512,2048]{2,1,0:T(8,128)(2,1)S(1)}, bf16[1,512,2048]{2,1,0:T(8,128)(2,1)}, u32[]{:S(2)}) copy-start(bf16[1,512,2048]{2,1,0:T(8,128)(2,1)} %param.29) | copy-start | bytes 6291460
  7.2 4.1 %copy-start.5 = (s32[128,2]{0,1:T(2,128)S(1)}, s32[128,2]{0,1:T(2,128)}, u32[]{:S(2)}) copy-start(s32[128,2]{0,1:T(2,128)} %param.24) | copy-start | bytes 3076
  7.2 5.7 %copy-start.1 = (bf16[128,2048]{1,0:T(8,128)(2,1)S(1)}, bf16[128,2048]{1,0:T(8,128)(2,1)}, u32[]{:S(2)}) copy-start(bf16[128,2048]{1,0:T(8,128)(2,1)} %param.22) | copy-start | bytes 1572868
  7.2 6.0 %copy-start.4 = (f32[2048]{0:T(1024)S(1)}, f32[2048]{0:T(1024)}, u32[]{:S(2)}) copy-start(f32[2048]{0:T(1024)} %param.23) | copy-start | bytes 24580
  7.2 61.6 %all-gather.5.cloned.1.call-start = ((), (), s32[]{:S(2)}) async-start(), calls=%async_computation.4 | async-start | bytes 1179648 | tf_op jit(solution)/shard_map/all_gather | solution.py:55
  10.5 100.7 %all-gather.3.cloned.1.call-start = ((), (), s32[]{:S(2)}) async-start(), calls=%async_computation.3 | async-start | bytes 1179648 | tf_op jit(solution)/shard_map/all_gather | solution.py:56
  20.4 7.7 %copy-start.2 = (bf16[512,256]{1,0:T(8,128)(2,1)S(1)}, bf16[512,256]{1,0:T(8,128)(2,1)}, u32[]{:S(2)}) copy-start(bf16[512,256]{1,0:T(8,128)(2,1)} %param.16) | copy-start | bytes 786436
  20.4 8.4 %copy-start.7 = (f32[128]{0:T(128)S(1)}, f32[128]{0:T(128)}, u32[]{:S(2)}) copy-start(f32[128]{0:T(128)} %param.19) | copy-start | bytes 1540
  20.4 112.2 %all-to-all-start = ((bf16[32,16,2048]{2,1,0:T(8,128)(2,1)}), bf16[32,16,2048]{2,1,0:T(8,128)(2,1)}, u32[]{:S(2)}, u32[]{:S(2)}) async-start(bf16[32,16,2048]{2,1,0:T(8,128)(2,1)} %bitcast.118), calls=%async_computation.1 | async-start | bytes 4194304 | tf_op jit(solution)/shard_map/all_to_all | solution.py:123
  143.3 52.3 %all-to-all-start.1 = ((bf16[32,16,2048]{2,1,0:T(8,128)(2,1)}), bf16[32,16,2048]{2,1,0:T(8,128)(2,1)}, u32[]{:S(2)}, u32[]{:S(2)}) async-start(bf16[32,16,2048]{2,1,0:T(8,128)(2,1)} %bitcast.119), calls=%async_computation.2 | async-start | bytes 4194304 | tf_op jit(solution)/shard_map/all_to_all | solution.py:133
  146.8 61.0 %reduce-scatter.2.cloned.1.call-start = ((), (), s32[]{:S(2)}) async-start(), calls=%async_computation.5 | async-start | bytes 2621440 | tf_op jit(solution)/shard_map/reduce_scatter | solution.py:85
  150.4 0.7 copy-start.3
  150.4 0.7 copy-start.6
Sparse Core Ops, SparseCore 0:
  10.7 58.1 all-gather.4
  71.0 40.2 all-gather.2
  150.7 36.8 reduce-scatter.1
where the time goes:
time: 215 us; the launch traced here: 214 us
  waiting for transfers between devices  125 us (58%)
  matrix products  35.1 us (16%)
  local copies, waits for them, and re-layouts  18.9 us (9%)
  between operations  14 us (7%)
  starting transfers between devices  11.5 us (5%)
  other arithmetic  9.72 us (5%)
    all_to_all x1, waiting for transfers between devices, expert_half(): lax.all_to_all(expert_out.reshape(device_count, capacity, model_width), (...  44.4 us
    all_gather x1, waiting for transfers between devices, attention_half(): value_piece = lax.all_gather(values, 'ep', axis=0, tiled=True)  40.1 us
    all_gather x1, waiting for transfers between devices, attention_half(): key_piece = lax.all_gather(krot, 'ep', axis=0, tiled=True)  39.7 us
    dot_general x4, matrix products, key_step(): jnp.einsum('qhgd,khd->qhgk', qrot, key_tile, preferred_element_type=jnp.f...  12.4 us
    dot_general x4, matrix products, key_step(): jnp.einsum('qhgk,khd->qhgd', weights, value_tile, preferred_element_type=...  8.77 us
    all_to_all x1, starting transfers between devices, expert_half(): lax.all_to_all(sender.reshape(device_count, capacity, model_width), ('ep'...  7.63 us
    scatter x1, local copies, waits for them, and re-layouts, expert_half(): sender = jnp.zeros((device_count * capacity, model_width), jnp.bfloat16)....  7 us
    dot_general x1, matrix products, expert_apply(): jnp.dot(hidden, down_w, preferred_element_type=jnp.float32)  6.21 us
  transfers between devices with their start and end apart: 5, of which 3 were waited for; matrix products, arithmetic and copies ran while one was open for 23% of the time, Pallas kernels for 0%

commit v1 on v0

--- a/solution.py
+++ b/solution.py
@@ -52,8 +52,11 @@
         jnp.zeros((row_count, local_kv, group_size, head_dim), jnp.float32),
         jnp.zeros((row_count, local_kv, group_size), jnp.float32),
     )
-    key_piece = lax.all_gather(krot, "ep", axis=0, tiled=True)
-    value_piece = lax.all_gather(values, "ep", axis=0, tiled=True)
+    key_piece, value_piece = jnp.split(
+        lax.all_gather(jnp.concatenate([krot, values], axis=1), "ep", axis=0, tiled=True),
+        [krot.shape[1]],
+        axis=1,
+    )
     piece_rows = key_piece.shape[0]
     key_block = math.gcd(piece_rows, 1024)
     block_count = piece_rows // key_block

time: 215 us -> 197 us (0.916)
  waiting for transfers between devices: 125 us -> 105 us
    all_gather x2 -> x1, waiting for transfers between devices: 79.8 us -> 60.9 us  [attention_half(): lax.all_gather(jnp.concatenate([krot, values], axis=1), 'ep', axis=0, til...]
    split x0 -> x1, local copies, waits for them, and re-layouts: none -> 3.02 us  [attention_half(): jnp.split(lax.all_gather(jnp.concatenate([krot, values], axis=1), 'ep', a...]
    unnamed x21 -> x22, local copies, waits for them, and re-layouts: 4.54 us -> 2.27 us
  transfers between devices with their start and end apart: 5 -> 4, of which waited for: 3 -> 2; matrix products, arithmetic and copies ran while one was open for 23% -> 25% of each run, Pallas kernels for 0% -> 0%
where the time goes in v1:
time: 197 us; the launch traced here: 196 us
  waiting for transfers between devices  105 us (53%)
  matrix products  35.1 us (18%)
  local copies, waits for them, and re-layouts  19.9 us (10%)
  between operations  14.4 us (7%)
  starting transfers between devices  11.4 us (6%)
  other arithmetic  9.91 us (5%)
    all_gather x1, waiting for transfers between devices, attention_half(): lax.all_gather(jnp.concatenate([krot, values], axis=1), 'ep', axis=0, til...  60.9 us
    all_to_all x1, waiting for transfers between devices, expert_half(): lax.all_to_all(expert_out.reshape(device_count, capacity, model_width), (...  44.4 us
    dot_general x4, matrix products, key_step(): jnp.einsum('qhgd,khd->qhgk', qrot, key_tile, preferred_element_type=jnp.f...  12.4 us
    dot_general x4, matrix products, key_step(): jnp.einsum('qhgk,khd->qhgd', weights, value_tile, preferred_element_type=...  8.77 us
    all_to_all x1, starting transfers between devices, expert_half(): lax.all_to_all(sender.reshape(device_count, capacity, model_width), ('ep'...  7.63 us
    scatter x1, local copies, waits for them, and re-layouts, expert_half(): sender = jnp.zeros((device_count * capacity, model_width), jnp.bfloat16)....  7 us
    dot_general x1, matrix products, expert_apply(): jnp.dot(hidden, down_w, preferred_element_type=jnp.float32)  6.21 us
    reduce_sum x1, other arithmetic, expert_half(): return jnp.sum(picked * combine[:, :, None], axis=1).astype(jnp.bfloat16)  5.59 us
  transfers between devices with their start and end apart: 4, of which 2 were waited for; matrix products, arithmetic and copies ran while one was open for 25% of the time, Pallas kernels for 0%

profile of v1, /device:TPU:0, one launch (start us, length us, event | category | flops | bytes accessed | tf_op | source)
XLA Modules:
  0.0 196.2 jit_solution(18151817092221372603)
XLA Ops:
  7.3 1.2 copy.31
  8.5 0.7 fusion.40
  10.1 0.9 pad_maximum_fusion
  13.1 7.0 %scatter_custom_fusion = bf16[512,2048]{1,0:T(8,128)(2,1)} fusion(s32[256]{0:T(256)S(1)} %bitcast.126, bf16[128,2048]{1,0:T(8,128)(2,1)S(1)} %fusion.28, s32[1024]{0:T(1024)S(1)} %pad_clamp_fusion.1, bf16[]{:T(256)} %constant.102.clone.1), kind=kCustom, calls=%fused_computation.32 | custom fusion | bytes 2097154 | tf_op jit(solution)/shard_map/scatter | solution.py:124
  20.1 7.6 %all-to-all-start = ((bf16[32,16,2048]{2,1,0:T(8,128)(2,1)}), bf16[32,16,2048]{2,1,0:T(8,128)(2,1)}, u32[]{:S(2)}, u32[]{:S(2)}) async-start(bf16[32,16,2048]{2,1,0:T(8,128)(2,1)} %bitcast.120), calls=%async_computation.1 | async-start | bytes 4194304 | tf_op jit(solution)/shard_map/all_to_all | solution.py:126
  28.9 60.9 %all-gather.2.cloned.1.call-done = bf16[4096,256]{1,0:T(8,128)(2,1)} async-done(((bf16[512,256]{1,0:T(8,128)(2,1)}), bf16[4096,256]{1,0:T(8,128)(2,1)}) %all-gather.2.cloned.1.call-update) | async-done | bytes 2097168 | tf_op jit(solution)/shard_map/all_gather | solution.py:56
  89.7 3.0 %fusion.63 = (bf16[4096,128]{1,0:T(8,128)(2,1)}, bf16[4096,128]{1,0:T(8,128)(2,1)}) fusion(bf16[4096,256]{1,0:T(8,128)(2,1)} %all-gather.2.cloned.1.call-done), kind=kLoop, calls=%fused_computation.106 | loop fusion | bytes 4194304 | tf_op jit(solution)/shard_map/split | solution.py:55
  92.8 21.3 %while.13 = (s32[]{:T(128)}, f32[512,1,2,128]{0,3,2,1:T(8,128)S(1)}, f32[512,1,2]{0,2,1:T(2,128)S(1)}, bf16[4,1024,1,128]{3,1,0,2:T(8,128)(2,1)}, bf16[4,1024,1,...) while((s32[]{:T(128)}, ...), condition=%wide.region_4.5_spmd.clone, body=%wide.region_2.4_spmd.clone.sunk | while | flops 541328384 | bytes 6046816 | solution.py:80
  92.8 3.1 %convert_reduce_fusion.2 = (f32[512,2]{0,1:T(2,128)S(1)}, bf16[1024,512,2]{1,0,2:T(8,128)(2,1)}) fusion(bf16[512,1,2,128]{3,0,2,1:T(8,128)(2,1)S(1)} %get-tuple-element.162, bf16[4,1024,1,128]{3,1,2,0:T(8,128)(2,1)} %get-tuple-element.161, s32[]{:T(128)} %get-tuple-element.149), kind=kOutput, calls=%fused_computation.3.clone.1 | convolution fusion | flops 272628736 | bytes 2626048 | tf_op jit(solution)/shard_map/while/body/eval_jaxpr/qhgd,khd->qhgk/dot_general | solution.py:70
  95.9 2.2 %fusion.72 = f32[512,1,2,128]{0,3,2,1:T(8,128)S(1)} fusion(bf16[1024,512,2]{1,0,2:T(8,128)(2,1)} %get-tuple-element.139, f32[512,1,2,128]{0,3,2,1:T(8,128)S(1)} %get-tuple-element.150, bf16[4,1024,1,128]{3,1,0,2:T(8,128)(2,1)} %get-tuple-element.160, s32[]{:T(128)} %get-tuple-element.149, pred[]{:T(512)S(6)} %compare.18), kind=kOutput, calls=%fused_computation.8.clone.1 | convolution fusion | flops 268697600 | bytes 3408385 | tf_op jit(solution)/shard_map/while/body/eval_jaxpr/qhgk,khd->qhgd/dot_general | solution.py:75
  98.1 3.1 %convert_reduce_fusion.2 = (f32[512,2]{0,1:T(2,128)S(1)}, bf16[1024,512,2]{1,0,2:T(8,128)(2,1)}) fusion(bf16[512,1,2,128]{3,0,2,1:T(8,128)(2,1)S(1)} %get-tuple-element.162, bf16[4,1024,1,128]{3,1,2,0:T(8,128)(2,1)} %get-tuple-element.161, s32[]{:T(128)} %get-tuple-element.149), kind=kOutput, calls=%fused_computation.3.clone.1 | convolution fusion | flops 272628736 | bytes 2626048 | tf_op jit(solution)/shard_map/while/body/eval_jaxpr/qhgd,khd->qhgk/dot_general | solution.py:70
  101.2 2.2 %fusion.72 = f32[512,1,2,128]{0,3,2,1:T(8,128)S(1)} fusion(bf16[1024,512,2]{1,0,2:T(8,128)(2,1)} %get-tuple-element.139, f32[512,1,2,128]{0,3,2,1:T(8,128)S(1)} %get-tuple-element.150, bf16[4,1024,1,128]{3,1,0,2:T(8,128)(2,1)} %get-tuple-element.160, s32[]{:T(128)} %get-tuple-element.149, pred[]{:T(512)S(6)} %compare.18), kind=kOutput, calls=%fused_computation.8.clone.1 | convolution fusion | flops 268697600 | bytes 3408385 | tf_op jit(solution)/shard_map/while/body/eval_jaxpr/qhgk,khd->qhgd/dot_general | solution.py:75
  103.4 3.1 %convert_reduce_fusion.2 = (f32[512,2]{0,1:T(2,128)S(1)}, bf16[1024,512,2]{1,0,2:T(8,128)(2,1)}) fusion(bf16[512,1,2,128]{3,0,2,1:T(8,128)(2,1)S(1)} %get-tuple-element.162, bf16[4,1024,1,128]{3,1,2,0:T(8,128)(2,1)} %get-tuple-element.161, s32[]{:T(128)} %get-tuple-element.149), kind=kOutput, calls=%fused_computation.3.clone.1 | convolution fusion | flops 272628736 | bytes 2626048 | tf_op jit(solution)/shard_map/while/body/eval_jaxpr/qhgd,khd->qhgk/dot_general | solution.py:70
  106.5 2.2 %fusion.72 = f32[512,1,2,128]{0,3,2,1:T(8,128)S(1)} fusion(bf16[1024,512,2]{1,0,2:T(8,128)(2,1)} %get-tuple-element.139, f32[512,1,2,128]{0,3,2,1:T(8,128)S(1)} %get-tuple-element.150, bf16[4,1024,1,128]{3,1,0,2:T(8,128)(2,1)} %get-tuple-element.160, s32[]{:T(128)} %get-tuple-element.149, pred[]{:T(512)S(6)} %compare.18), kind=kOutput, calls=%fused_computation.8.clone.1 | convolution fusion | flops 268697600 | bytes 3408385 | tf_op jit(solution)/shard_map/while/body/eval_jaxpr/qhgk,khd->qhgd/dot_general | solution.py:75
  108.8 3.1 %convert_reduce_fusion.2 = (f32[512,2]{0,1:T(2,128)S(1)}, bf16[1024,512,2]{1,0,2:T(8,128)(2,1)}) fusion(bf16[512,1,2,128]{3,0,2,1:T(8,128)(2,1)S(1)} %get-tuple-element.162, bf16[4,1024,1,128]{3,1,2,0:T(8,128)(2,1)} %get-tuple-element.161, s32[]{:T(128)} %get-tuple-element.149), kind=kOutput, calls=%fused_computation.3.clone.1 | convolution fusion | flops 272628736 | bytes 2626048 | tf_op jit(solution)/shard_map/while/body/eval_jaxpr/qhgd,khd->qhgk/dot_general | solution.py:70
  111.9 2.2 %fusion.72 = f32[512,1,2,128]{0,3,2,1:T(8,128)S(1)} fusion(bf16[1024,512,2]{1,0,2:T(8,128)(2,1)} %get-tuple-element.139, f32[512,1,2,128]{0,3,2,1:T(8,128)S(1)} %get-tuple-element.150, bf16[4,1024,1,128]{3,1,0,2:T(8,128)(2,1)} %get-tuple-element.160, s32[]{:T(128)} %get-tuple-element.149, pred[]{:T(512)S(6)} %compare.18), kind=kOutput, calls=%fused_computation.8.clone.1 | convolution fusion | flops 268697600 | bytes 3408385 | tf_op jit(solution)/shard_map/while/body/eval_jaxpr/qhgk,khd->qhgd/dot_general | solution.py:75
  114.2 4.4 %fusion.18 = f32[512,512]{1,0:T(8,128)} fusion(bf16[512,2048]{1,0:T(8,128)(2,1)} %bitcast.19, bf16[1,2048,512]{2,1,0:T(8,128)(2,1)} %param.27), kind=kOutput, calls=%fused_computation.22 | convolution fusion | flops 1073741824 | bytes 5242880 | tf_op jit(solution)/shard_map/dot_general | solution.py:97
  118.6 6.2 %convolution_convert_fusion.1 = bf16[512,2048]{1,0:T(8,128)(2,1)} fusion(bf16[1,512,2048]{2,1,0:T(8,128)(2,1)S(1)} %copy-done, bf16[512,2048]{1,0:T(8,128)(2,1)} %bitcast.19, bf16[1,2048,512]{2,1,0:T(8,128)(2,1)} %param.28, f32[512,512]{1,0:T(8,128)} %fusion.18), kind=kOutput, calls=%fused_computation.18 | convolution fusion | flops 2150105088 | bytes 9437184 | tf_op jit(solution)/shard_map/dot_general | solution.py:100
  124.8 3.5 %all-to-all-start.1 = ((bf16[32,16,2048]{2,1,0:T(8,128)(2,1)}), bf16[32,16,2048]{2,1,0:T(8,128)(2,1)}, u32[]{:S(2)}, u32[]{:S(2)}) async-start(bf16[32,16,2048]{2,1,0:T(8,128)(2,1)} %bitcast.122), calls=%async_computation.2 | async-start | bytes 4194304 | tf_op jit(solution)/shard_map/all_to_all | solution.py:136
  128.6 3.3 %convolution_convert_fusion = bf16[512,2048]{1,0:T(8,128)(2,1)} fusion(bf16[512,256]{0,1:T(8,128)(2,1)S(1)} %bitcast.123, bf16[1024,2048]{1,0:T(8,128)(2,1)} %param.21, s32[]{:T(128)S(6)} %select_n.58), kind=kOutput, calls=%fused_computation.17 | convolution fusion | flops 537919488 | bytes 3407876 | tf_op jit(solution)/shard_map/dot_general | solution.py:89
  132.8 44.4 %all-to-all-done.1 = bf16[32,16,2048]{2,1,0:T(8,128)(2,1)} async-done(((bf16[32,16,2048]{2,1,0:T(8,128)(2,1)}), bf16[32,16,2048]{2,1,0:T(8,128)(2,1)}, u32[]{:S(2)}, u32[]{:S(2)}) %all-to-all-start.1) | async-done | bytes 2097184 | tf_op jit(solution)/shard_map/all_to_all | solution.py:136
  177.2 4.2 %gather_fusion = bf16[256,2048]{1,0:T(8,128)(2,1)S(1)} fusion(bf16[512,2048]{1,0:T(8,128)(2,1)} %bitcast.24, s32[1024]{0:T(1024)S(1)} %pad_clamp_fusion), kind=kCustom, calls=%fused_computation.1 | custom fusion | bytes 2098176 | tf_op jit(solution)/shard_map/gather | solution.py:144
  181.4 2.3 %reshape.420 = f32[128,2,2048]{2,1,0:T(2,128)} reshape(bf16[256,2048]{1,0:T(8,128)(2,1)S(1)} %gather_fusion) | data formatting | bytes 3145728 | tf_op jit(solution)/shard_map/convert_element_type | solution.py:144
  183.8 5.6 %multiply_reduce_fusion = bf16[128,2048]{1,0:T(8,128)(2,1)} fusion(f32[128,2,2048]{2,1,0:T(2,128)} %reshape.420, f32[128,2]{1,0:T(8,128)S(1)} %copy.42), kind=kLoop, calls=%fused_computation.24 | loop fusion | flops 786432 | bytes 2622464 | tf_op jit(solution)/shard_map/reduce_sum | solution.py:146
  (70 shorter events, 5.2 us)
Async XLA Ops:
  7.2 111.4 %copy-start = (bf16[1,512,2048]{2,1,0:T(8,128)(2,1)S(1)}, bf16[1,512,2048]{2,1,0:T(8,128)(2,1)}, u32[]{:S(2)}) copy-start(bf16[1,512,2048]{2,1,0:T(8,128)(2,1)} %param.29) | copy-start | bytes 6291460
  7.2 2.9 %copy-start.3 = (bf16[512,128]{1,0:T(8,128)(2,1)S(1)}, bf16[512,128]{1,0:T(8,128)(2,1)}, u32[]{:S(2)}) copy-start(bf16[512,128]{1,0:T(8,128)(2,1)} %param.18) | copy-start | bytes 393220
  7.2 3.8 %copy-start.6 = (s32[128,2]{0,1:T(2,128)S(1)}, s32[128,2]{0,1:T(2,128)}, u32[]{:S(2)}) copy-start(s32[128,2]{0,1:T(2,128)} %param.24) | copy-start | bytes 3076
  7.2 5.5 %copy-start.1 = (bf16[128,2048]{1,0:T(8,128)(2,1)S(1)}, bf16[128,2048]{1,0:T(8,128)(2,1)}, u32[]{:S(2)}) copy-start(bf16[128,2048]{1,0:T(8,128)(2,1)} %param.22) | copy-start | bytes 1572868
  7.2 5.7 %copy-start.5 = (f32[2048]{0:T(1024)S(1)}, f32[2048]{0:T(1024)}, u32[]{:S(2)}) copy-start(f32[2048]{0:T(1024)} %param.23) | copy-start | bytes 24580
  7.2 82.5 %all-gather.2.cloned.1.call-start = ((), (), s32[]{:S(2)}) async-start(), calls=%async_computation.3 | async-start | bytes 2359296 | tf_op jit(solution)/shard_map/all_gather | solution.py:56
  20.1 7.7 %copy-start.2 = (bf16[512,256]{1,0:T(8,128)(2,1)S(1)}, bf16[512,256]{1,0:T(8,128)(2,1)}, u32[]{:S(2)}) copy-start(bf16[512,256]{1,0:T(8,128)(2,1)} %param.16) | copy-start | bytes 786436
  20.1 8.4 %copy-start.8 = (f32[128]{0:T(128)S(1)}, f32[128]{0:T(128)}, u32[]{:S(2)}) copy-start(f32[128]{0:T(128)} %param.19) | copy-start | bytes 1540
  20.1 94.1 %all-to-all-start = ((bf16[32,16,2048]{2,1,0:T(8,128)(2,1)}), bf16[32,16,2048]{2,1,0:T(8,128)(2,1)}, u32[]{:S(2)}, u32[]{:S(2)}) async-start(bf16[32,16,2048]{2,1,0:T(8,128)(2,1)} %bitcast.120), calls=%async_computation.1 | async-start | bytes 4194304 | tf_op jit(solution)/shard_map/all_to_all | solution.py:126
  124.8 52.4 %all-to-all-start.1 = ((bf16[32,16,2048]{2,1,0:T(8,128)(2,1)}), bf16[32,16,2048]{2,1,0:T(8,128)(2,1)}, u32[]{:S(2)}, u32[]{:S(2)}) async-start(bf16[32,16,2048]{2,1,0:T(8,128)(2,1)} %bitcast.122), calls=%async_computation.2 | async-start | bytes 4194304 | tf_op jit(solution)/shard_map/all_to_all | solution.py:136
  128.3 61.0 %reduce-scatter.2.cloned.1.call-start = ((), (), s32[]{:S(2)}) async-start(), calls=%async_computation.4 | async-start | bytes 2621440 | tf_op jit(solution)/shard_map/reduce_scatter | solution.py:88
  131.9 0.7 copy-start.4
  131.9 0.7 copy-start.7
Sparse Core Ops, SparseCore 0:
  11.1 78.5 all-gather.1
  132.2 36.7 reduce-scatter.1
